TPU v7x, 32 devices: a whole 2x2x4 slice. The times are simulated.
32 devices in a mesh: ep: 8 (over z, core), tp: 4 (over y, x).
Axes of the slice: x: 2, y: 2, z: 4, core: 2. Of those that a mesh axis runs over, the one named last changes fastest.
Arguments:
- tokens: bfloat16 [1024, 2048], P('ep', 'tp'), may hold values from -6 to 6
- owner_shard: int32 [32768, 1], P('ep'), may hold values from 0 to 7; in each aligned block of 4096 rows (0 to 4095, 4096 to 8191, ...) at most 1024 rows name the same one
- local_row: int32 [32768, 1], P('ep'), may hold values from 0 to 4095
- gate_weights: float32 [1024, 32], P('ep'), may hold values from 0.05 to 1
- up_table: bfloat16 [32768, 2048], P('ep', 'tp'), may hold values from -0.125 to 0.125
- down_table: bfloat16 [32768, 2048], P('ep', 'tp'), may hold values from -6 to 6
Outputs:
- mixed: bfloat16 [1024, 2048], P('ep', 'tp')
Inputs may be any that keep to these rules, and one draw needn't show every extreme that they name: `owner_shard`: within the rows of one device (128 tokens of 32 slots each, token by token) no shard is named by more than 1024 slots, a bound that some block reaches; every shard is named somewhere.
All inputs are finite; a program needn't handle non-finite values.
Results may differ from a plain program's by a relative error of at most 0.0049.
Values may be sent and summed in bfloat16 or wider, within the bound.
A program may use at most 128 MiB of HBM per device.

v0:
```python
import jax
import jax.numpy as jnp
from jax import lax
from jax.sharding import PartitionSpec as P


def bucket_slots(holders, targets, capacity):
    pair_count = holders.shape[0]
    target_count = targets.shape[0]
    matches = (holders[:, None] == targets[None, :]).astype(jnp.int32)
    ranking = jnp.cumsum(matches, 0) - 1
    position = jnp.sum(ranking * matches, 1)
    target_of = jnp.sum(matches * jnp.arange(target_count, dtype=jnp.int32)[None, :], 1)
    present = jnp.sum(matches, 1) > 0
    flat_slot = jnp.where(present, target_of * capacity + position, target_count * capacity)
    slot_table = jnp.full((target_count * capacity + 1,), pair_count, jnp.int32)
    slot_table = slot_table.at[flat_slot].set(jnp.arange(pair_count, dtype=jnp.int32))
    slot_index = slot_table[: target_count * capacity].reshape(target_count, capacity)
    return (slot_index, slot_index < pair_count)


def serve_requests(got_rows, got_local, got_token, got_gate, up_table, down_table, tok_dev):
    up_rows = up_table[got_local]
    products = jnp.einsum("scw,scw->sc", up_rows, got_rows, preferred_element_type=jnp.float32)
    products = lax.psum(products, "tp")
    weighted = (got_gate * jax.nn.gelu(products)).astype(jnp.bfloat16)
    selector = got_token[:, None, :] == jnp.arange(tok_dev, dtype=jnp.int32)[None, :, None]
    spread_weight = jnp.where(selector, weighted[:, None, :], jnp.zeros((), jnp.bfloat16))
    down_rows = down_table[got_local]
    return jnp.einsum("stc,scw->stw", spread_weight, down_rows, preferred_element_type=jnp.float32)


def on_device(tokens, owner_shard, local_row, gate_weights, up_table, down_table):
    ep_count = lax.axis_size("ep")
    tok_dev, columns = tokens.shape
    slot_count = gate_weights.shape[1]
    pair_count = tok_dev * slot_count
    capacity = 2 * pair_count // ep_count
    owner_flat = owner_shard[:, 0]
    row_flat = local_row[:, 0]
    gate_flat = gate_weights.reshape(pair_count)
    targets = jnp.arange(ep_count, dtype=jnp.int32)
    slot_index, valid = bucket_slots(owner_flat, targets, capacity)
    clipped = jnp.minimum(slot_index, pair_count - 1)
    token_of = clipped // slot_count
    send_rows = tokens[token_of]
    send_ints = jnp.stack([row_flat[clipped], token_of], 1)
    send_gate = jnp.where(valid, gate_flat[clipped], jnp.float32(0.0))
    got_rows = lax.all_to_all(send_rows, "ep", split_axis=0, concat_axis=0, tiled=True)
    got_ints, got_gate = (
        lax.all_to_all(send_ints, "ep", split_axis=0, concat_axis=0, tiled=True),
        lax.all_to_all(send_gate, "ep", split_axis=0, concat_axis=0, tiled=True),
    )
    partial_value = serve_requests(
        got_rows, got_ints[:, 0], got_ints[:, 1], got_gate, up_table, down_table, tok_dev
    )
    returned = lax.all_to_all(partial_value, "ep", split_axis=0, concat_axis=0, tiled=True)
    combined = jnp.sum(returned, 0)
    return combined.astype(jnp.bfloat16)


def solution(mesh):
    return jax.shard_map(
        on_device,
        mesh=mesh,
        in_specs=(
            P("ep", "tp"),
            P("ep", None),
            P("ep", None),
            P("ep", None),
            P("ep", "tp"),
            P("ep", "tp"),
        ),
        out_specs=P("ep", "tp"),
        check_vma=False,
    )
```

profile of v0, /device:TPU:0, one launch (start us, length us, event | category | flops | bytes accessed | tf_op | source)
XLA Modules:
  0.0 383.1 jit_solution(9205955504624490228)
XLA Ops:
  0.0 0.0 copy-start
  0.0 0.0 copy-start.1
  0.0 0.8 fusion.9
  0.8 2.3 reduce-window.6
  3.1 0.3 slice_reduce_fusion
  3.4 0.2 reduce-window.9
  3.6 0.1 add_bitcast_fusion
  3.7 0.9 convert_reduce_fusion
  4.7 15.5 %scatter_custom_fusion = s32[8193]{0:T(1024)S(1)} fusion(s32[4096]{0:T(1024)S(1)} %bitcast.56, s32[4096]{0:T(1024)S(1)} %iota.16, s32[]{:T(128)} %constant.17.clone.1), kind=kCustom, calls=%fused_computation.51 | custom fusion | bytes 32776 | tf_op jit(solution)/shard_map/scatter | solution.py:17
  20.2 0.1 and_select_fusion.1
  20.4 0.2 compare_select_fusion
  20.6 0.0 copy-done.1
  20.6 45.5 %gather_fusion = s32[8192]{0:T(1024)S(1)} fusion(s32[4096]{0:T(1024)S(1)} %bitcast.41, s32[8192]{0:T(1024)S(1)} %broadcast_clamp_fusion.2), kind=kCustom, calls=%fused_computation | custom fusion | bytes 98304 | tf_op jit(solution)/shard_map/gather | solution.py:47
  66.1 0.7 pad_add_fusion
  66.8 6.4 %all-to-all-start = ((s32[8,2,1024]{2,1,0:T(2,128)}), s32[8,2,1024]{2,1,0:T(2,128)S(1)}, u32[]{:S(2)}, u32[]{:S(2)}) async-start(s32[8,2,1024]{2,1,0:T(2,128)} %pad_add_fusion), calls=%async_computation | async-start | bytes 131072 | tf_op jit(solution)/shard_map/all_to_all | solution.py:51
  73.2 0.0 copy-done
  73.2 33.6 %gather_fusion.3 = bf16[8192,512]{1,0:T(8,128)(2,1)} fusion(bf16[128,512]{1,0:T(8,128)(2,1)S(1)} %copy-done, s32[8192]{0:T(1024)S(1)} %broadcast_clamp_fusion), kind=kCustom, calls=%fused_computation.3 | custom fusion | bytes 16809984 | tf_op jit(solution)/shard_map/gather | solution.py:46
  106.8 0.0 all-to-all-done
  106.8 0.0 copy-start.2
  106.8 5.2 %all-to-all-start.2 = ((bf16[8,1024,512]{2,1,0:T(8,128)(2,1)}), bf16[8,1024,512]{2,1,0:T(8,128)(2,1)}, u32[]{:S(2)}, u32[]{:S(2)}) async-start(bf16[8,1024,512]{2,1,0:T(8,128)(2,1)} %bitcast.42), calls=%async_computation.2 | async-start | bytes 16777216 | tf_op jit(solution)/shard_map/all_to_all | solution.py:49
  112.0 0.0 copy-done.2
  112.0 0.1 copy.8
  112.1 0.1 reshape.246
  112.2 45.5 %gather_fusion.1 = f32[8192]{0:T(1024)S(1)} fusion(f32[4096]{0:T(1024)S(1)} %reshape.246, s32[8192]{0:T(1024)S(1)} %broadcast_clamp_fusion.2), kind=kCustom, calls=%fused_computation.1 | custom fusion | bytes 98304 | tf_op jit(solution)/shard_map/gather | solution.py:48
  157.7 0.6 compare_select_fusion.10
  158.5 36.5 %gather_fusion.4 = bf16[8192,512]{1,0:T(8,128)(2,1)} fusion(bf16[4096,512]{1,0:T(8,128)(2,1)} %param.11, s32[8192]{0:T(1024)S(1)} %broadcast_clamp_fusion.1), kind=kCustom, calls=%fused_computation.4 | custom fusion | bytes 16809984 | tf_op jit(solution)/shard_map/gather | solution.py:29
  195.0 36.5 %gather_fusion.2 = bf16[8192,512]{1,0:T(8,128)(2,1)} fusion(bf16[4096,512]{1,0:T(8,128)(2,1)} %param.10, s32[8192]{0:T(1024)S(1)} %broadcast_clamp_fusion.1), kind=kCustom, calls=%fused_computation.2 | custom fusion | bytes 16809984 | tf_op jit(solution)/shard_map/gather | solution.py:23
  231.5 64.5 %all-to-all-done.2 = bf16[8,1024,512]{2,1,0:T(8,128)(2,1)} async-done(((bf16[8,1024,512]{2,1,0:T(8,128)(2,1)}), bf16[8,1024,512]{2,1,0:T(8,128)(2,1)}, u32[]{:S(2)}, u32[]{:S(2)}) %all-to-all-start.2) | async-done | bytes 8388640 | tf_op jit(solution)/shard_map/all_to_all | solution.py:49
  296.0 3.3 all-to-all-start.1
  299.3 8.0 %fusion = f32[8,1024]{1,0:T(8,128)S(1)} fusion(bf16[8,1024,512]{2,1,0:T(8,128)(2,1)} %bitcast.43, bf16[8,1024,512]{2,1,0:T(8,128)(2,1)} %all-to-all-done.2), kind=kLoop, calls=%fused_computation.7 | loop fusion | flops 16769024 | bytes 16809984 | tf_op jit(solution)/shard_map/scw,scw->sc/dot_general | solution.py:24
  307.3 16.3 %psum.7 = f32[8,1024]{1,0:T(8,128)S(1)} all-reduce(f32[8,1024]{1,0:T(8,128)S(1)} %fusion), channel_id=1, replica_groups=mesh['ep'=8,'tp'=4] {'tp'}, use_global_device_ids=true, to_apply=%region_6.7 | all-reduce | flops 8192 | bytes 65536 | tf_op jit(solution)/shard_map/psum | solution.py:25
  323.6 0.0 all-to-all-done.1
  323.7 4.6 %fusion.2 = f32[8,128,512]{2,1,0:T(8,128)S(1)} fusion(bf16[8,1024,512]{2,1,0:T(8,128)(2,1)} %bitcast.44, s32[8,1024]{1,0:T(8,128)S(1)} %bitcast.54, bf16[8,1024]{1,0:T(8,128)(2,1)S(1)} %fusion.18), kind=kOutput, calls=%fused_computation.10 | convolution fusion | flops 1075838976 | bytes 10534912 | tf_op jit(solution)/shard_map/stc,scw->stw/dot_general | solution.py:30
  328.3 53.9 %all_to_all.24 = f32[8,128,512]{2,1,0:T(8,128)S(1)} all-to-all(f32[8,128,512]{2,1,0:T(8,128)S(1)} %fusion.2), channel_id=1, replica_groups=mesh['ep'=8,'tp'=4] {'ep'}, dimensions={0} | all-to-all | bytes 4194304 | tf_op jit(solution)/shard_map/all_to_all | solution.py:57
  382.2 0.9 reduce_sum.39
  (11 shorter events, 0.2 us)
Async XLA Ops:
  0.0 73.2 %copy-start = (bf16[128,512]{1,0:T(8,128)(2,1)S(1)}, bf16[128,512]{1,0:T(8,128)(2,1)}, u32[]{:S(2)}) copy-start(bf16[128,512]{1,0:T(8,128)(2,1)} %param.6) | copy-start | bytes 393220
  0.0 20.6 %copy-start.1 = (s32[4096,1]{0,1:T(1,128)S(1)}, s32[4096,1]{0,1:T(1,128)}, u32[]{:S(2)}) copy-start(s32[4096,1]{0,1:T(1,128)} %param.8) | copy-start | bytes 49156
  66.8 39.9 %all-to-all-start = ((s32[8,2,1024]{2,1,0:T(2,128)}), s32[8,2,1024]{2,1,0:T(2,128)S(1)}, u32[]{:S(2)}, u32[]{:S(2)}) async-start(s32[8,2,1024]{2,1,0:T(2,128)} %pad_add_fusion), calls=%async_computation | async-start | bytes 131072 | tf_op jit(solution)/shard_map/all_to_all | solution.py:51
  106.8 5.2 %copy-start.2 = (f32[128,32]{0,1:T(8,128)S(1)}, f32[128,32]{0,1:T(8,128)}, u32[]{:S(2)}) copy-start(f32[128,32]{0,1:T(8,128)} %param.9) | copy-start | bytes 49156
  106.8 189.2 %all-to-all-start.2 = ((bf16[8,1024,512]{2,1,0:T(8,128)(2,1)}), bf16[8,1024,512]{2,1,0:T(8,128)(2,1)}, u32[]{:S(2)}, u32[]{:S(2)}) async-start(bf16[8,1024,512]{2,1,0:T(8,128)(2,1)} %bitcast.42), calls=%async_computation.2 | async-start | bytes 16777216 | tf_op jit(solution)/shard_map/all_to_all | solution.py:49
  296.0 27.7 %all-to-all-start.1 = ((f32[8,1,1024]{2,1,0:T(1,128)}), f32[8,1,1024]{2,1,0:T(1,128)S(1)}, u32[]{:S(2)}, u32[]{:S(2)}) async-start(f32[8,1,1024]{2,1,0:T(1,128)} %bitcast.10), calls=%async_computation.1 | async-start | bytes 65536 | tf_op jit(solution)/shard_map/all_to_all | solution.py:52
where the time goes:
time: 384 us; the launch traced here: 383 us
  local copies, waits for them, and re-layouts  214 us (56%)
  blocking collectives  70.2 us (18%)
  waiting for transfers between devices  64.5 us (17%)
  other arithmetic  15 us (4%)
  starting transfers between devices  14.9 us (4%)
  matrix products  4.65 us (1%)
    all_to_all x1, waiting for transfers between devices, on_device(): lax.all_to_all(send_rows, 'ep', split_axis=0, concat_axis=0, tiled=True)  64.5 us
    all_to_all x1, blocking collectives, on_device(): lax.all_to_all(partial_value, 'ep', split_axis=0, concat_axis=0, tiled=True)  53.9 us
    gather x1, local copies, waits for them, and re-layouts, on_device(): send_gate = jnp.where(valid, gate_flat[clipped], jnp.float32(0.0))  45.5 us
    gather x1, local copies, waits for them, and re-layouts, on_device(): send_ints = jnp.stack([row_flat[clipped], token_of], 1)  45.5 us
    gather x1, local copies, waits for them, and re-layouts, serve_requests(): up_rows = up_table[got_local]  36.5 us
    gather x1, local copies, waits for them, and re-layouts, serve_requests(): down_rows = down_table[got_local]  36.5 us
    gather x1, local copies, waits for them, and re-layouts, on_device(): send_rows = tokens[token_of]  33.6 us
    psum x1, blocking collectives, serve_requests(): products = lax.psum(products, 'tp')  16.3 us
  transfers between devices with their start and end apart: 3, of which 1 were waited for; matrix products, arithmetic and copies ran while one was open for 42% of the time, Pallas kernels for 0%

commit v1 on v0

v1 whole, which is shorter than its diff:
```python
import functools

import jax
import jax.numpy as jnp
from jax import lax
from jax.experimental import pallas as pl
from jax.experimental.pallas import tpu as pltpu
from jax.sharding import PartitionSpec as P

MESH = pl.DeviceIdType.MESH
VMEM_BYTES = 60 * 1024 * 1024


def params(number):
    return pltpu.CompilerParams(
        collective_id=number, has_side_effects=True, vmem_limit_bytes=VMEM_BYTES
    )


def vmem():
    return pl.BlockSpec(memory_space=pltpu.VMEM)


def greet(peers):
    barrier = pltpu.get_barrier_semaphore()
    for peer in peers:
        pl.semaphore_signal(barrier, inc=1, device_id=peer, device_id_type=MESH)
    pl.semaphore_wait(barrier, len(peers))


def remote(src, dst, send_sem, recv_sem, peer):
    return pltpu.make_async_remote_copy(
        src_ref=src, dst_ref=dst, send_sem=send_sem, recv_sem=recv_sem,
        device_id=peer, device_id_type=MESH,
    )


def gather_kernel(n_ep, tok_ref, aux_ref, all_tok, all_aux, local_sem, send, recv, fsend, frecv):
    chips = n_ep // 2
    me = lax.axis_index("ep")
    core = lax.rem(me, 2)
    chip = me // 2
    partner = {"ep": me + 1 - 2 * core}

    def at(step):
        return lax.rem(chip + step, chips) * 2 + core

    greet([partner] + [{"ep": at(d)} for d in range(1, chips)])
    pairs = ((tok_ref, all_tok), (aux_ref, all_aux))
    started = []
    for d in range(1, chips):
        for i, (src, dst) in enumerate(pairs):
            copy = remote(src, dst.at[me], send.at[i, d], recv.at[i, d], {"ep": at(d)})
            copy.start()
            started.append(copy)
    local = []
    for i, (src, dst) in enumerate(pairs):
        copy = remote(src, dst.at[me], fsend.at[i, 0], frecv.at[i, 0], partner)
        copy.start()
        started.append(copy)
        own = pltpu.make_async_copy(src, dst.at[me], local_sem.at[i])
        own.start()
        local.append(own)
    for d in range(1, chips):
        source = at(chips - d)
        for i, (src, dst) in enumerate(pairs):
            remote(src, dst.at[source], send.at[i, d], recv.at[i, d], partner).wait_recv()
            copy = remote(dst.at[source], dst.at[source], fsend.at[i, d], frecv.at[i, d], partner)
            copy.start()
            started.append(copy)
    for d in range(chips):
        source = at(chips - d) + 1 - 2 * core
        for i, (src, dst) in enumerate(pairs):
            remote(src, dst.at[source], fsend.at[i, d], frecv.at[i, d], partner).wait_recv()
    for copy in local:
        copy.wait()
    for copy in started:
        copy.wait_send()


def up_kernel(slots, tok_ref, ids_ref, up_hbm, out_ref, up_buf, hi_ref, lo_ref, acc_ref, sems):
    experts, width = up_hbm.shape
    chunks = up_buf.shape[0]
    rows = up_buf.shape[1]
    for c in range(chunks):
        pltpu.make_async_copy(up_hbm.at[pl.ds(c * rows, rows)], up_buf.at[c], sems.at[c]).start()
    blocks = tok_ref.shape[0]
    first = lax.axis_index("ep") * experts
    group = ids_ref.shape[1]
    segments = tok_ref.shape[1] // group
    per_tile = 128 // slots
    lane = lax.broadcasted_iota(jnp.int32, (group, 128), 1) // slots

    def prepare(b, carry):
        for k in range(segments):
            half = k // per_tile
            local = ids_ref[b, :, half * 128:(half + 1) * 128].astype(jnp.int32) - first
            fits = (local >= 0) & (local < experts) & (lane == k % per_tile)
            where = pl.ds(pl.multiple_of((b * segments + k) * group, group), group)
            hi_ref[where, :] = jnp.where(fits, local // 128, -1)
            lo_ref[where, :] = local & 127
        return carry

    lax.fori_loop(0, blocks, prepare, 0)
    acc_ref[...] = jnp.zeros_like(acc_ref)
    tokens = tok_ref.shape[0] * tok_ref.shape[1]

    def step(c, carry):
        pltpu.make_async_copy(up_hbm.at[pl.ds(c * rows, rows)], up_buf.at[c], sems.at[c]).wait()
        product = lax.dot_general(
            tok_ref[...].reshape(tokens, width), up_buf[c], (((1,), (1,)), ((), ())),
            preferred_element_type=jnp.float32,
        )
        acc = acc_ref[...]
        hi = hi_ref[...]
        lo = lo_ref[...]
        for i in range(rows // 128):
            picked = jnp.take_along_axis(
                product[:, i * 128:(i + 1) * 128], lo, axis=1, mode="promise_in_bounds"
            )
            acc = jnp.where(hi == c * (rows // 128) + i, picked, acc)
        acc_ref[...] = acc
        return carry

    lax.fori_loop(0, chunks, step, 0)

    def pack(b, carry):
        halves = []
        for half in range(segments // per_tile):
            total = None
            for k in range(half * per_tile, (half + 1) * per_tile):
                part = acc_ref[pl.ds(pl.multiple_of((b * segments + k) * group, group), group), :]
                total = part if total is None else total + part
            halves.append(total)
        out_ref[pl.ds(pl.multiple_of(b * group, group), group), :] = jnp.concatenate(halves, axis=1)
        return carry

    lax.fori_loop(0, blocks, pack, 0)


def weight_kernel(n_tp, prod_ref, gate_ref, out_ref, got, send, recv, wsend, wrecv):
    me = lax.axis_index("tp")
    rows = prod_ref.shape[0] // n_tp

    def span(q):
        return pl.ds(pl.multiple_of(q * rows, rows), rows)

    def at(step):
        return lax.rem(me + step, n_tp)

    greet([{"tp": at(d)} for d in range(1, n_tp)])
    started = []
    for d in range(1, n_tp):
        copy = remote(prod_ref.at[span(at(d))], got.at[d - 1], send.at[d], recv.at[d], {"tp": at(d)})
        copy.start()
        started.append(copy)
    total = prod_ref[span(me), :]
    for d, copy in enumerate(started):
        copy.wait_recv()
        total += got[d]
    out_ref[span(me), :] = (gate_ref[span(me), :] * jax.nn.gelu(total)).astype(jnp.bfloat16)
    for d in range(1, n_tp):
        copy = remote(out_ref.at[span(me)], out_ref.at[span(me)], wsend.at[d], wrecv.at[d], {"tp": at(d)})
        copy.start()
        started.append(copy)
    for d in range(1, n_tp):
        source = span(at(n_tp - d))
        remote(out_ref.at[source], out_ref.at[source], wsend.at[d], wrecv.at[d], {"tp": at(d)}).wait_recv()
    for copy in started:
        copy.wait_send()


def down_kernel(n_ep, slots, wts_ref, ids_ref, down_hbm, out_ref, down_buf, w_ref, own, xbuf, ybuf,
                sbuf, rbuf, dsem, xsend, xrecv, send, recv):
    chips = n_ep // 2
    me = lax.axis_index("ep")
    core = lax.rem(me, 2)
    chip = me // 2
    partner = {"ep": me + 1 - 2 * core}
    load = pltpu.make_async_copy(down_hbm, down_buf, dsem)
    load.start()

    def at(step):
        return lax.rem(chip + step, chips)

    greet([partner] + [{"ep": at(d) * 2 + core} for d in range(1, chips)])
    experts = down_hbm.shape[0]
    tiles = experts // 128
    first = me * experts
    group = ids_ref.shape[1]
    lanes = ids_ref.shape[2]
    tokens = lanes // slots
    block = group * tokens
    row_key = lax.broadcasted_iota(jnp.int32, (tiles * tokens, lanes), 0)
    low_key = lax.broadcasted_iota(jnp.int32, (128, lanes), 0)
    turn = lax.broadcasted_iota(jnp.int32, (1, lanes), 1) // slots

    def spread(b, j):
        local = ids_ref[b, pl.ds(j, 1), :].astype(jnp.int32) - first
        weight = wts_ref[b, pl.ds(j, 1), :]
        fits = (local >= 0) & (local < experts)
        key = jnp.where(fits, (local // 128) * tokens + turn, -1)
        left = jnp.where(row_key == key, weight, 0.0).astype(jnp.bfloat16)
        right = jnp.where(low_key == (local & 127), 1.0, 0.0).astype(jnp.bfloat16)
        wide = lax.dot_general(left, right, (((1,), (1,)), ((), ())), preferred_element_type=jnp.float32)
        return wide.reshape(tiles, tokens, 128)

    loaded = False
    copies = []

    def finish(i):
        d = i + 1
        copies[i].wait_recv()
        sbuf[i] = (own[i] + ybuf[i].astype(jnp.float32)).astype(jnp.bfloat16)
        copy = remote(sbuf.at[i], rbuf.at[i], send.at[i], recv.at[i], {"ep": at(d) * 2 + core})
        copy.start()
        return copy

    sent = []
    for i in range(chips):
        target = at(i + 1)

        def build(x, carry):
            b = target * 2 + x // (group // 2)
            j = lax.rem(x, group // 2) * 2
            both = jnp.concatenate([spread(b, j), spread(b, j + 1)], axis=1).astype(jnp.bfloat16)
            for h in range(tiles):
                w_ref[pl.ds(pl.multiple_of(x * 16, 16), 16), h * 128:(h + 1) * 128] = both[h]
            return carry

        lax.fori_loop(0, group, build, 0)
        if not loaded:
            load.wait()
            loaded = True
        part = jnp.dot(w_ref[...], down_buf[...], preferred_element_type=jnp.float32)
        low, high = part[:block], part[block:]
        mine = jnp.where(core == 0, low, high)
        other = jnp.where(core == 0, high, low)
        own[i] = mine
        xbuf[i] = other.astype(jnp.bfloat16)
        copy = remote(xbuf.at[i], ybuf.at[i], xsend.at[i], xrecv.at[i], partner)
        copy.start()
        copies.append(copy)
        if i > 0:
            sent.append(finish(i - 1))
    last = chips - 1
    copies[last].wait_recv()
    total = own[last] + ybuf[last].astype(jnp.float32)
    for i, copy in enumerate(sent):
        copy.wait_recv()
        total += rbuf[i].astype(jnp.float32)
    out_ref[...] = total.astype(jnp.bfloat16)
    for copy in copies + sent:
        copy.wait_send()


def on_device(tokens, owner_shard, local_row, gate_weights, up_table, down_table):
    n_ep, n_tp = lax.axis_size("ep"), lax.axis_size("tp")
    count, width = tokens.shape
    slots = gate_weights.shape[1]
    experts = up_table.shape[0]
    side = 8
    group, lanes = count // side, side * slots
    chips = n_ep // 2
    shuffled = tokens.reshape(group, side, width).transpose(1, 0, 2).reshape(count, width)
    ids = owner_shard[:, 0] * experts + local_row[:, 0]
    aux = jnp.stack([ids.astype(jnp.float32).reshape(group, lanes), gate_weights.reshape(group, lanes)])
    dma = pltpu.SemaphoreType.DMA
    all_tok, all_aux = pl.pallas_call(
        functools.partial(gather_kernel, n_ep),
        out_shape=(
            jax.ShapeDtypeStruct((n_ep, count, width), jnp.bfloat16),
            jax.ShapeDtypeStruct((n_ep, 2, group, lanes), jnp.float32),
        ),
        in_specs=[vmem()] * 2,
        out_specs=(vmem(), vmem()),
        scratch_shapes=[dma((2,)), dma((2, chips)), dma((2, chips)), dma((2, chips)), dma((2, chips))],
        compiler_params=params(0),
        name="gather_tokens",
    )(shuffled, aux)
    all_ids = all_aux[:, 0]
    gates = all_aux[:, 1].reshape(n_ep * group, lanes)
    total = n_ep * count
    chunks = 16
    products = pl.pallas_call(
        functools.partial(up_kernel, slots),
        out_shape=jax.ShapeDtypeStruct((n_ep * group, lanes), jnp.float32),
        in_specs=[vmem(), vmem(), pl.BlockSpec(memory_space=pl.ANY)],
        out_specs=vmem(),
        scratch_shapes=[
            pltpu.VMEM((chunks, experts // chunks, width), jnp.bfloat16),
            pltpu.VMEM((total, 128), jnp.int32),
            pltpu.VMEM((total, 128), jnp.int32),
            pltpu.VMEM((total, 128), jnp.float32),
            dma((chunks,)),
        ],
        compiler_params=pltpu.CompilerParams(vmem_limit_bytes=VMEM_BYTES),
        name="up_products",
    )(all_tok, all_ids, up_table)
    weights = pl.pallas_call(
        functools.partial(weight_kernel, n_tp),
        out_shape=jax.ShapeDtypeStruct((n_ep * group, lanes), jnp.bfloat16),
        in_specs=[vmem()] * 2,
        out_specs=vmem(),
        scratch_shapes=[
            pltpu.VMEM((n_tp - 1, n_ep * group // n_tp, lanes), jnp.float32),
            dma((n_tp,)), dma((n_tp,)), dma((n_tp,)), dma((n_tp,)),
        ],
        compiler_params=params(1),
        name="slot_weights",
    )(products, gates)
    weights = weights.astype(jnp.float32).reshape(n_ep, group, lanes)
    return pl.pallas_call(
        functools.partial(down_kernel, n_ep, slots),
        out_shape=jax.ShapeDtypeStruct((count, width), jnp.bfloat16),
        in_specs=[vmem(), vmem(), pl.BlockSpec(memory_space=pl.ANY)],
        out_specs=vmem(),
        scratch_shapes=[
            pltpu.VMEM((experts, width), jnp.bfloat16),
            pltpu.VMEM((2 * count, experts), jnp.bfloat16),
            pltpu.VMEM((chips, count, width), jnp.float32),
            pltpu.VMEM((chips, count, width), jnp.bfloat16),
            pltpu.VMEM((chips, count, width), jnp.bfloat16),
            pltpu.VMEM((chips, count, width), jnp.bfloat16),
            pltpu.VMEM((chips, count, width), jnp.bfloat16),
            dma, dma((chips,)), dma((chips,)), dma((chips,)), dma((chips,)),
        ],
        compiler_params=params(2),
        name="down_sums",
    )(weights, all_ids, down_table)


def solution(mesh):
    return jax.shard_map(
        on_device,
        mesh=mesh,
        in_specs=(
            P("ep", "tp"),
            P("ep", None),
            P("ep", None),
            P("ep", None),
            P("ep", "tp"),
            P("ep", "tp"),
        ),
        out_specs=P("ep", "tp"),
        check_vma=False,
    )
```

time: 384 us -> 90 us (0.23)
  local copies, waits for them, and re-layouts: 214 us -> 6.36 us
  Pallas kernels: 0 us -> 80.3 us
  blocking collectives: 70.2 us -> 0 us
  waiting for transfers between devices: 64.5 us -> 0 us
  starting transfers between devices: 14.9 us -> 0 us
  other arithmetic: 15 us -> 2.88 us
  matrix products: 4.65 us -> 0 us
    gather x5 -> x0, local copies, waits for them, and re-layouts: 198 us -> none  [the longest x1 45.5 us: on_device(): send_gate = jnp.where(valid, gate_flat[clipped], jnp.float32(0.0))]
    pallas_call x0 -> x4, Pallas kernels: none -> 80.3 us  [the longest x1 31.3 us: on_device(): pl.pallas_call(functools.partial(down_kernel, n_ep, slots), out_shape=jax...]
    all_to_all x3 -> x0, waiting for transfers between devices: 64.5 us -> none  [the longest x1 64.5 us: on_device(): lax.all_to_all(send_rows, 'ep', split_axis=0, concat_axis=0, tiled=True)]
    all_to_all x1 -> x0, blocking collectives: 53.9 us -> none  [on_device(): lax.all_to_all(partial_value, 'ep', split_axis=0, concat_axis=0, tiled=True)]
    psum x1 -> x0, blocking collectives: 16.3 us -> none  [serve_requests(): products = lax.psum(products, 'tp')]
    scatter x1 -> x0, local copies, waits for them, and re-layouts: 15.5 us -> none  [bucket_slots(): slot_table.at[flat_slot].set(jnp.arange(pair_count, dtype=jnp.int32))]
    all_to_all x3 -> x0, starting transfers between devices: 14.9 us -> none  [the longest x1 6.35 us: on_device(): lax.all_to_all(send_ints, 'ep', split_axis=0, concat_axis=0, tiled=True)]
    dot_general x1 -> x0, other arithmetic: 8.04 us -> none  [serve_requests(): jnp.einsum('scw,scw->sc', up_rows, got_rows, preferred_element_type=jnp.f...]
  transfers between devices with their start and end apart: 3 -> 0, of which waited for: 1 -> 0; matrix products, arithmetic and copies ran while one was open for 42% -> 0% of each run, Pallas kernels for 0% -> 0%
where the time goes in v1:
time: 90 us; the launch traced here: 89.6 us
  Pallas kernels  80.3 us (89%)
  local copies, waits for them, and re-layouts  6.36 us (7%)
  other arithmetic  2.88 us (3%)
    pallas_call x1, Pallas kernels, on_device(): pl.pallas_call(functools.partial(down_kernel, n_ep, slots), out_shape=jax...  31.3 us
    pallas_call x1, Pallas kernels, on_device(): pl.pallas_call(functools.partial(gather_kernel, n_ep), out_shape=(jax.Sha...  20.4 us
    pallas_call x1, Pallas kernels, on_device(): pl.pallas_call(functools.partial(up_kernel, slots), out_shape=jax.ShapeDt...  17.4 us
    pallas_call x1, Pallas kernels, on_device(): pl.pallas_call(functools.partial(weight_kernel, n_tp), out_shape=jax.Shap...  11.2 us
    unnamed x4, local copies, waits for them, and re-layouts  2.39 us

profile of v1, /device:TPU:0, one launch (start us, length us, event | category | flops | bytes accessed | tf_op | source)
XLA Modules:
  0.0 89.6 jit_solution(17499873426083656377)
XLA Ops:
  0.0 0.8 convert_reduce_fusion
  0.8 0.8 copy.11
  1.6 0.1 stack_reshape.4
  1.7 0.6 pad_maximum_fusion.aux_ref
  2.3 1.6 %copy.10 = bf16[16,8,512]{2,0,1:T(8,128)(2,1)} copy(bf16[16,8,512]{2,1,0:T(8,128)(2,1)} %bitcast.12) | data formatting | bytes 262144 | tf_op jit(solution)/shard_map/reshape | solution.py:265
  3.9 20.4 %gather_tokens.1 = (bf16[8,128,512]{2,1,0:T(8,128)(2,1)}, f32[8,2,16,256]{3,2,1,0:T(8,128)}) custom-call(bf16[128,512]{1,0:T(8,128)(2,1)} %bitcast.9, f32[2,16,256]{2,1,0:T(8,128)} %pad_maximum_fusion.aux_ref), custom_call_target="tpu_custom_call" | custom-call | tf_op jit(solution)/shard_map/gather_tokens/pallas_call | solution.py:269
  24.4 0.0 copy-start
  24.4 1.6 %slice_bitcast_fusion.ids_ref = f32[8,16,256]{2,1,0:T(8,128)} fusion(f32[8,2,16,256]{3,2,1,0:T(8,128)} %get-tuple-element.8), kind=kLoop, calls=%fused_computation | loop fusion | bytes 262144 | tf_op jit(solution)/shard_map/squeeze | solution.py:281
  26.0 17.4 %up_products.1.prod_ref = f32[128,256]{1,0:T(8,128)} custom-call(bf16[8,128,512]{2,1,0:T(8,128)(2,1)} %get-tuple-element.7.tok_ref, f32[8,16,256]{2,1,0:T(8,128)} %slice_bitcast_fusion.ids_ref, bf16[4096,512]{1,0:T(8,128)(2,1)} %up_hbm.1), custom_call_target="tpu_custom_call" | custom-call | tf_op jit(solution)/shard_map/up_products/pallas_call | solution.py:285
  43.4 0.0 copy-done
  43.4 0.6 slice.7
  44.0 11.2 %slot_weights.1 = bf16[128,256]{1,0:T(8,128)(2,1)} custom-call(f32[128,256]{1,0:T(8,128)} %up_products.1.prod_ref, f32[128,256]{1,0:T(8,128)} %bitcast.10), custom_call_target="tpu_custom_call" | custom-call | tf_op jit(solution)/shard_map/slot_weights/pallas_call | solution.py:300
  55.3 1.5 %convert.1.wts_ref = f32[8,16,256]{2,1,0:T(8,128)} convert(bf16[8,16,256]{2,1,0:T(8,128)(2,1)} %bitcast.11) | non-fusion elementwise | flops 32768 | bytes 196608 | tf_op jit(solution)/shard_map/reshape | solution.py:312
  56.7 31.3 %down_sums.1 = bf16[128,512]{1,0:T(8,128)(2,1)} custom-call(f32[8,16,256]{2,1,0:T(8,128)} %convert.1.wts_ref, f32[8,16,256]{2,1,0:T(8,128)} %slice_bitcast_fusion.ids_ref, bf16[4096,512]{1,0:T(8,128)(2,1)} %down_hbm.1), custom_call_target="tpu_custom_call" | custom-call | tf_op jit(solution)/shard_map/down_sums/pallas_call | solution.py:313
  88.0 1.6 %copy.16 = bf16[128,512]{1,0:T(8,128)(2,1)} copy(bf16[128,512]{1,0:T(8,128)(2,1)} %down_sums.1) | data formatting | bytes 262144
  (1 shorter events, 0.0 us)
Async XLA Ops:
  24.4 19.0 %copy-start = (f32[8,2,16,256]{3,2,1,0:T(8,128)S(1)}, f32[8,2,16,256]{3,2,1,0:T(8,128)}, u32[]{:S(2)}) copy-start(f32[8,2,16,256]{3,2,1,0:T(8,128)} %get-tuple-element.8) | copy-start | bytes 786436

commit v2 on v0

v2 whole, which is shorter than its diff:
```python
import functools

import jax
import jax.numpy as jnp
from jax import lax
from jax.experimental import pallas as pl
from jax.experimental.pallas import tpu as pltpu
from jax.sharding import PartitionSpec as P

MESH = pl.DeviceIdType.MESH
VMEM_BYTES = 60 * 1024 * 1024


def params(number):
    return pltpu.CompilerParams(
        collective_id=number, has_side_effects=True, vmem_limit_bytes=VMEM_BYTES
    )


def vmem():
    return pl.BlockSpec(memory_space=pltpu.VMEM)


def greet(peers):
    barrier = pltpu.get_barrier_semaphore()
    for peer in peers:
        pl.semaphore_signal(barrier, inc=1, device_id=peer, device_id_type=MESH)
    pl.semaphore_wait(barrier, len(peers))


def remote(src, dst, send_sem, recv_sem, peer):
    return pltpu.make_async_remote_copy(
        src_ref=src, dst_ref=dst, send_sem=send_sem, recv_sem=recv_sem,
        device_id=peer, device_id_type=MESH,
    )


def fused_kernel(n_ep, n_tp, slots, tok_ref, aux_ref, up_hbm, down_hbm, out_ref,
                 all_tok, all_aux, up_buf, down_buf, hi_ref, lo_ref, acc_ref, pbuf, pgot, wt_ref, w_ref,
                 own, xbuf, ybuf, sbuf, rbuf,
                 local_sem, send, recv, fsend, frecv, up_sem, down_sem, psend, precv,
                 xsend, xrecv, rsend, rrecv):
    chips = n_ep // 2
    me = lax.axis_index("ep")
    core = lax.rem(me, 2)
    chip = me // 2
    part = lax.axis_index("tp")
    partner = {"ep": me + 1 - 2 * core}
    experts, width = up_hbm.shape
    chunks, chunk_rows = up_buf.shape[0], up_buf.shape[1]
    tiles = experts // 128
    first = me * experts
    group, lanes = aux_ref.shape[1], aux_ref.shape[2]
    side = lanes // slots
    block = group * side
    per_tile = 128 // slots

    def at(step):
        return lax.rem(chip + step, chips)

    def counterpart(step):
        return {"ep": at(step) * 2 + core}

    def tp_peer(step):
        return {"tp": lax.rem(part + step, n_tp)}

    up_loads = []
    for c in range(chunks):
        load = pltpu.make_async_copy(up_hbm.at[pl.ds(c * chunk_rows, chunk_rows)], up_buf.at[c], up_sem.at[c])
        load.start()
        up_loads.append(load)
    greet([partner] + [counterpart(d) for d in range(1, chips)] + [tp_peer(d) for d in range(1, n_tp)])

    pairs = ((aux_ref, all_aux), (tok_ref, all_tok))
    started = []
    local = []
    for i, (src, dst) in enumerate(pairs):
        own_copy = pltpu.make_async_copy(src, dst.at[me], local_sem.at[i])
        own_copy.start()
        local.append(own_copy)
        copy = remote(src, dst.at[me], fsend.at[i, 0], frecv.at[i, 0], partner)
        copy.start()
        started.append(copy)
    for d in range(1, chips):
        for i, (src, dst) in enumerate(pairs):
            copy = remote(src, dst.at[me], send.at[i, d], recv.at[i, d], counterpart(d))
            copy.start()
            started.append(copy)
    down_load = pltpu.make_async_copy(down_hbm, down_buf, down_sem)
    down_load.start()

    def forward(d):
        source = at(chips - d) * 2 + core
        for i, (src, dst) in enumerate(pairs):
            remote(src, dst.at[source], send.at[i, d], recv.at[i, d], partner).wait_recv()
            copy = remote(dst.at[source], dst.at[source], fsend.at[i, d], frecv.at[i, d], partner)
            copy.start()
            started.append(copy)

    def arrive(d):
        source = at(chips - d) * 2 + 1 - core
        for i, (src, dst) in enumerate(pairs):
            remote(src, dst.at[source], fsend.at[i, d], frecv.at[i, d], partner).wait_recv()

    lane = lax.broadcasted_iota(jnp.int32, (group, 128), 1) // slots

    def up_step(d, base):
        for b in range(2):
            for k in range(side):
                half = k // per_tile
                here = all_aux[base + b, 0, :, half * 128:(half + 1) * 128].astype(jnp.int32) - first
                fits = (here >= 0) & (here < experts) & (lane == k % per_tile)
                where = pl.ds(b * block + k, group, stride=side)
                hi_ref[where, :] = jnp.where(fits, here // 128, -1)
                lo_ref[where, :] = here & 127
        acc_ref[...] = jnp.zeros_like(acc_ref)
        if d == 0:
            for load in up_loads:
                load.wait()

        def chunk(c, carry):
            product = lax.dot_general(
                all_tok[pl.ds(base, 2)].reshape(2 * block, width), up_buf[c], (((1,), (1,)), ((), ())),
                preferred_element_type=jnp.float32,
            )
            acc = acc_ref[...]
            hi = hi_ref[...]
            lo = lo_ref[...]
            for i in range(chunk_rows // 128):
                picked = jnp.take_along_axis(
                    product[:, i * 128:(i + 1) * 128], lo, axis=1, mode="promise_in_bounds"
                )
                acc = jnp.where(hi == c * (chunk_rows // 128) + i, picked, acc)
            acc_ref[...] = acc
            return carry

        lax.fori_loop(0, chunks, chunk, 0)
        for b in range(2):
            for half in range(side // per_tile):
                total = None
                for k in range(half * per_tile, (half + 1) * per_tile):
                    piece = acc_ref[pl.ds(b * block + k, group, stride=side), :]
                    total = piece if total is None else total + piece
                pbuf[d, b, :, half * 128:(half + 1) * 128] = total
        copies = []
        for t in range(1, n_tp):
            copy = remote(pbuf.at[d], pgot.at[d, t], psend.at[d, t], precv.at[d, t], tp_peer(t))
            copy.start()
            copies.append(copy)
        started.extend(copies)
        return copies

    row_key = lax.broadcasted_iota(jnp.int32, (tiles * side, lanes), 0)
    low_key = lax.broadcasted_iota(jnp.int32, (128, lanes), 0)
    turn = lax.broadcasted_iota(jnp.int32, (1, lanes), 1) // slots

    def down_step(d, base, copies):
        total = pbuf[d]
        for t, copy in enumerate(copies):
            copy.wait_recv()
            total += pgot[d, t + 1]
        gate = all_aux[pl.ds(base, 2), 1]
        wt_ref[...] = (gate * jax.nn.gelu(total)).astype(jnp.bfloat16).astype(jnp.float32)

        def spread(b, j):
            here = all_aux[base + b, 0, pl.ds(j, 1), :].astype(jnp.int32) - first
            weight = wt_ref[b, pl.ds(j, 1), :]
            fits = (here >= 0) & (here < experts)
            key = jnp.where(fits, (here // 128) * side + turn, -1)
            left = jnp.where(row_key == key, weight, 0.0).astype(jnp.bfloat16)
            right = jnp.where(low_key == (here & 127), 1.0, 0.0).astype(jnp.bfloat16)
            wide = lax.dot_general(left, right, (((1,), (1,)), ((), ())), preferred_element_type=jnp.float32)
            return wide.reshape(tiles, side, 128)

        def build(x, carry):
            b = x // (group // 2)
            j = lax.rem(x, group // 2) * 2
            both = jnp.concatenate([spread(b, j), spread(b, j + 1)], axis=1).astype(jnp.bfloat16)
            for h in range(tiles):
                w_ref[pl.ds(pl.multiple_of(x * 2 * side, 2 * side), 2 * side), h * 128:(h + 1) * 128] = both[h]
            return carry

        lax.fori_loop(0, group, build, 0)
        if d == 0:
            down_load.wait()
        sums = jnp.dot(w_ref[...], down_buf[...], preferred_element_type=jnp.float32)
        low, high = sums[:block], sums[block:]
        own[d] = jnp.where(core == 0, low, high)
        xbuf[d] = jnp.where(core == 0, high, low).astype(jnp.bfloat16)
        copy = remote(xbuf.at[d], ybuf.at[d], xsend.at[d], xrecv.at[d], partner)
        copy.start()
        started.append(copy)
        return copy

    returned = []

    def finish(d, copy):
        copy.wait_recv()
        if d == 0:
            return
        sbuf[d] = (own[d] + ybuf[d].astype(jnp.float32)).astype(jnp.bfloat16)
        copy = remote(sbuf.at[d], rbuf.at[d], rsend.at[d], rrecv.at[d], counterpart(chips - d))
        copy.start()
        returned.append(copy)

    def base_of(d):
        return at(chips - d) * 2 if d else chip * 2

    for copy in local:
        copy.wait()
    waiting = None
    exchanged = None
    for d in range(chips + 1):
        if d < chips:
            arrive(d)
            sending = up_step(d, base_of(d))
            if d + 1 < chips:
                forward(d + 1)
        else:
            sending = None
        if d > 0:
            copy = down_step(d - 1, base_of(d - 1), waiting)
            if exchanged is not None:
                finish(d - 2, exchanged)
            exchanged = copy
        waiting = sending
    finish(chips - 1, exchanged)
    total = own[0] + ybuf[0].astype(jnp.float32)
    for d, copy in enumerate(returned):
        copy.wait_recv()
        total += rbuf[d + 1].astype(jnp.float32)
    out_ref[...] = total.astype(jnp.bfloat16)
    for copy in started + returned:
        copy.wait_send()


def on_device(tokens, owner_shard, local_row, gate_weights, up_table, down_table):
    n_ep, n_tp = lax.axis_size("ep"), lax.axis_size("tp")
    count, width = tokens.shape
    slots = gate_weights.shape[1]
    experts = up_table.shape[0]
    side = 8
    group, lanes = count // side, side * slots
    chips = n_ep // 2
    ids = owner_shard[:, 0] * experts + local_row[:, 0]
    aux = jnp.stack([ids.astype(jnp.float32).reshape(group, lanes), gate_weights.reshape(group, lanes)])
    dma = pltpu.SemaphoreType.DMA
    chunks = experts // 512
    wide = (chips, count, width)
    anywhere = pl.BlockSpec(memory_space=pl.ANY)
    return pl.pallas_call(
        functools.partial(fused_kernel, n_ep, n_tp, slots),
        out_shape=jax.ShapeDtypeStruct((count, width), jnp.bfloat16),
        in_specs=[vmem(), vmem(), anywhere, anywhere],
        out_specs=vmem(),
        scratch_shapes=[
            pltpu.VMEM((n_ep, count, width), jnp.bfloat16),
            pltpu.VMEM((n_ep, 2, group, lanes), jnp.float32),
            pltpu.VMEM((chunks, experts // chunks, width), jnp.bfloat16),
            pltpu.VMEM((experts, width), jnp.bfloat16),
            pltpu.VMEM((2 * count, 128), jnp.int32),
            pltpu.VMEM((2 * count, 128), jnp.int32),
            pltpu.VMEM((2 * count, 128), jnp.float32),
            pltpu.VMEM((chips, 2, group, lanes), jnp.float32),
            pltpu.VMEM((chips, n_tp, 2, group, lanes), jnp.float32),
            pltpu.VMEM((2, group, lanes), jnp.float32),
            pltpu.VMEM((2 * count, experts), jnp.bfloat16),
            pltpu.VMEM(wide, jnp.float32),
            pltpu.VMEM(wide, jnp.bfloat16),
            pltpu.VMEM(wide, jnp.bfloat16),
            pltpu.VMEM(wide, jnp.bfloat16),
            pltpu.VMEM(wide, jnp.bfloat16),
            dma((2,)), dma((2, chips)), dma((2, chips)), dma((2, chips)), dma((2, chips)),
            dma((chunks,)), dma, dma((chips, n_tp)), dma((chips, n_tp)),
            dma((chips,)), dma((chips,)), dma((chips,)), dma((chips,)),
        ],
        compiler_params=params(0),
        name="retrieve",
    )(tokens, aux, up_table, down_table)


def solution(mesh):
    return jax.shard_map(
        on_device,
        mesh=mesh,
        in_specs=(
            P("ep", "tp"),
            P("ep", None),
            P("ep", None),
            P("ep", None),
            P("ep", "tp"),
            P("ep", "tp"),
        ),
        out_specs=P("ep", "tp"),
        check_vma=False,
    )
```

time: 384 us -> 68.3 us (0.18)
  local copies, waits for them, and re-layouts: 214 us -> 2.47 us
  blocking collectives: 70.2 us -> 0 us
  waiting for transfers between devices: 64.5 us -> 0 us
  Pallas kernels: 0 us -> 64 us
  starting transfers between devices: 14.9 us -> 0 us
  other arithmetic: 15 us -> 1.41 us
  matrix products: 4.65 us -> 0 us
    gather x5 -> x0, local copies, waits for them, and re-layouts: 198 us -> none  [the longest x1 45.5 us: on_device(): send_gate = jnp.where(valid, gate_flat[clipped], jnp.float32(0.0))]
    all_to_all x3 -> x0, waiting for transfers between devices: 64.5 us -> none  [the longest x1 64.5 us: on_device(): lax.all_to_all(send_rows, 'ep', split_axis=0, concat_axis=0, tiled=True)]
    pallas_call x0 -> x1, Pallas kernels: none -> 64 us  [on_device(): pl.pallas_call(functools.partial(fused_kernel, n_ep, n_tp, slots), out_sh...]
    all_to_all x1 -> x0, blocking collectives: 53.9 us -> none  [on_device(): lax.all_to_all(partial_value, 'ep', split_axis=0, concat_axis=0, tiled=True)]
    psum x1 -> x0, blocking collectives: 16.3 us -> none  [serve_requests(): products = lax.psum(products, 'tp')]
    scatter x1 -> x0, local copies, waits for them, and re-layouts: 15.5 us -> none  [bucket_slots(): slot_table.at[flat_slot].set(jnp.arange(pair_count, dtype=jnp.int32))]
    all_to_all x3 -> x0, starting transfers between devices: 14.9 us -> none  [the longest x1 6.35 us: on_device(): lax.all_to_all(send_ints, 'ep', split_axis=0, concat_axis=0, tiled=True)]
    dot_general x1 -> x0, other arithmetic: 8.04 us -> none  [serve_requests(): jnp.einsum('scw,scw->sc', up_rows, got_rows, preferred_element_type=jnp.f...]
  transfers between devices with their start and end apart: 3 -> 0, of which waited for: 1 -> 0; matrix products, arithmetic and copies ran while one was open for 42% -> 0% of each run, Pallas kernels for 0% -> 0%
where the time goes in v2:
time: 68.3 us; the launch traced here: 67.9 us
  Pallas kernels  64 us (94%)
  local copies, waits for them, and re-layouts  2.47 us (4%)
  other arithmetic  1.41 us (2%)
    pallas_call x1, Pallas kernels, on_device(): pl.pallas_call(functools.partial(fused_kernel, n_ep, n_tp, slots), out_sh...  64 us
    unnamed x2, local copies, waits for them, and re-layouts  2.38 us

profile of v2, /device:TPU:0, one launch (start us, length us, event | category | flops | bytes accessed | tf_op | source)
XLA Modules:
  0.0 67.9 jit_solution(14583856419348170724)
XLA Ops:
  0.0 0.8 %convert_reduce_fusion = f32[4096]{0:T(1024)S(1)} fusion(s32[4096,1]{0,1:T(1,128)} %param.8, s32[4096,1]{0,1:T(1,128)} %param.7), kind=kLoop, calls=%fused_computation.1 | loop fusion | flops 12288 | bytes 49152 | tf_op jit(solution)/shard_map/convert_element_type | solution.py:246
  0.8 0.8 %copy.8 = f32[128,32]{1,0:T(8,128)S(1)} copy(f32[128,32]{0,1:T(8,128)} %param.9) | data formatting | bytes 32768 | tf_op args[3]
  1.6 0.1 stack_reshape.4
  1.7 0.6 pad_maximum_fusion.aux_ref
  2.3 64.0 %retrieve.1 = bf16[128,512]{1,0:T(8,128)(2,1)} custom-call(bf16[128,512]{1,0:T(8,128)(2,1)} %tok_ref.1, f32[2,16,256]{2,1,0:T(8,128)} %pad_maximum_fusion.aux_ref, bf16[4096,512]{1,0:T(8,128)(2,1)} %up_hbm.1, bf16[4096,512]{1,0:T(8,128)(2,1)} %down_hbm.1), custom_call_target="tpu_custom_call" | custom-call | tf_op jit(solution)/shard_map/retrieve/pallas_call | solution.py:251
  66.3 1.6 %copy.10 = bf16[128,512]{1,0:T(8,128)(2,1)} copy(bf16[128,512]{1,0:T(8,128)(2,1)} %retrieve.1) | data formatting | bytes 262144
  (1 shorter events, 0.0 us)

commit v3 on v2

--- a/solution.py
+++ b/solution.py
@@ -134,7 +134,7 @@
             acc_ref[...] = acc
             return carry
 
-        lax.fori_loop(0, chunks, chunk, 0)
+        lax.fori_loop(0, chunks, chunk, 0, unroll=4)
         for b in range(2):
             for half in range(side // per_tile):
                 total = None
@@ -150,9 +150,18 @@
         started.extend(copies)
         return copies
 
-    row_key = lax.broadcasted_iota(jnp.int32, (tiles * side, lanes), 0)
-    low_key = lax.broadcasted_iota(jnp.int32, (128, lanes), 0)
-    turn = lax.broadcasted_iota(jnp.int32, (1, lanes), 1) // slots
+    def row_keys(count):
+        keys = lax.broadcasted_iota(jnp.int32, (count, lanes), 0).astype(jnp.float32)
+        return keys.astype(jnp.bfloat16).reshape(count // 16, 16, lanes)
+
+    row_key = row_keys(tiles * side)
+    low_key = row_keys(128)
+    turn = lax.broadcasted_iota(jnp.int32, (16, lanes), 1) // slots
+    zero = jnp.zeros((1, 16, lanes), jnp.bfloat16)
+    one = jnp.ones((1, 16, lanes), jnp.bfloat16)
+
+    def narrow(x):
+        return x.astype(jnp.float32).astype(jnp.bfloat16)[None]
 
     def down_step(d, base, copies):
         total = pbuf[d]
@@ -163,12 +172,12 @@
         wt_ref[...] = (gate * jax.nn.gelu(total)).astype(jnp.bfloat16).astype(jnp.float32)
 
         def spread(b, j):
-            here = all_aux[base + b, 0, pl.ds(j, 1), :].astype(jnp.int32) - first
-            weight = wt_ref[b, pl.ds(j, 1), :]
+            here = jnp.broadcast_to(all_aux[base + b, 0, pl.ds(j, 1), :], (16, lanes)).astype(jnp.int32) - first
+            weight = jnp.broadcast_to(wt_ref[b, pl.ds(j, 1), :], (16, lanes)).astype(jnp.bfloat16)[None]
             fits = (here >= 0) & (here < experts)
-            key = jnp.where(fits, (here // 128) * side + turn, -1)
-            left = jnp.where(row_key == key, weight, 0.0).astype(jnp.bfloat16)
-            right = jnp.where(low_key == (here & 127), 1.0, 0.0).astype(jnp.bfloat16)
+            key = narrow(jnp.where(fits, (here // 128) * side + turn, -1))
+            left = jnp.where(row_key == key, weight, zero).reshape(tiles * side, lanes)
+            right = jnp.where(low_key == narrow(here & 127), one, zero).reshape(128, lanes)
             wide = lax.dot_general(left, right, (((1,), (1,)), ((), ())), preferred_element_type=jnp.float32)
             return wide.reshape(tiles, side, 128)
 
@@ -180,7 +189,7 @@
                 w_ref[pl.ds(pl.multiple_of(x * 2 * side, 2 * side), 2 * side), h * 128:(h + 1) * 128] = both[h]
             return carry
 
-        lax.fori_loop(0, group, build, 0)
+        lax.fori_loop(0, group, build, 0, unroll=4)
         if d == 0:
             down_load.wait()
         sums = jnp.dot(w_ref[...], down_buf[...], preferred_element_type=jnp.float32)

time: 68.3 us -> 56.6 us (0.83)
  Pallas kernels: 64 us -> 52.3 us
    pallas_call x1, Pallas kernels: 64 us -> 52.3 us  [on_device(): pl.pallas_call(functools.partial(fused_kernel, n_ep, n_tp, slots), out_sh...]
where the time goes in v3:
time: 56.6 us; the launch traced here: 56.2 us
  Pallas kernels  52.3 us (92%)
  local copies, waits for them, and re-layouts  2.47 us (4%)
  other arithmetic  1.41 us (2%)
    pallas_call x1, Pallas kernels, on_device(): pl.pallas_call(functools.partial(fused_kernel, n_ep, n_tp, slots), out_sh...  52.3 us
    unnamed x2, local copies, waits for them, and re-layouts  2.38 us

profile of v3, /device:TPU:0, one launch (start us, length us, event | category | flops | bytes accessed | tf_op | source)
XLA Modules:
  0.0 56.2 jit_solution(5917816636185155493)
XLA Ops:
  0.0 0.8 %convert_reduce_fusion = f32[4096]{0:T(1024)S(1)} fusion(s32[4096,1]{0,1:T(1,128)} %param.8, s32[4096,1]{0,1:T(1,128)} %param.7), kind=kLoop, calls=%fused_computation.1 | loop fusion | flops 12288 | bytes 49152 | tf_op jit(solution)/shard_map/convert_element_type | solution.py:255
  0.8 0.8 %copy.8 = f32[128,32]{1,0:T(8,128)S(1)} copy(f32[128,32]{0,1:T(8,128)} %param.9) | data formatting | bytes 32768 | tf_op args[3]
  1.6 0.1 stack_reshape.4
  1.7 0.6 %pad_maximum_fusion.aux_ref = f32[2,16,256]{2,1,0:T(8,128)} fusion(f32[1,16,256]{2,1,0:T(8,128)S(1)} %stack_reshape.4, f32[1,16,256]{2,1,0:T(8,128)S(1)} %convert_element_type.14), kind=kLoop, calls=%fused_computation | loop fusion | flops 8192 | bytes 65536 | tf_op jit(solution)/shard_map/stack | solution.py:255
  2.3 52.3 %retrieve.1 = bf16[128,512]{1,0:T(8,128)(2,1)} custom-call(bf16[128,512]{1,0:T(8,128)(2,1)} %tok_ref.1, f32[2,16,256]{2,1,0:T(8,128)} %pad_maximum_fusion.aux_ref, bf16[4096,512]{1,0:T(8,128)(2,1)} %up_hbm.1, bf16[4096,512]{1,0:T(8,128)(2,1)} %down_hbm.1), custom_call_target="tpu_custom_call" | custom-call | tf_op jit(solution)/shard_map/retrieve/pallas_call | solution.py:260
  54.6 1.6 %copy.10 = bf16[128,512]{1,0:T(8,128)(2,1)} copy(bf16[128,512]{1,0:T(8,128)(2,1)} %retrieve.1) | data formatting | bytes 262144
  (1 shorter events, 0.0 us)
